TPU v7x, 512 devices: a whole 4x8x8 slice. The times are simulated.
512 devices in a mesh: ep: 128 (over z, y, core), tp: 4 (over x).
Axes of the slice: x: 4, y: 8, z: 8, core: 2. Of those that a mesh axis runs over, the one named last changes fastest.
Arguments:
- tokens: bfloat16 [2048, 1024], P(('ep', 'tp')), may hold values from -6 to 6
- gain_attn: bfloat16 [1024], replicated, may hold values from 0.099609375 to 1.8984375
- gain_ffn: bfloat16 [1024], replicated, may hold values from 0.099609375 to 1.8984375
- w_query: bfloat16 [1024, 512], P(None, 'tp'), may hold values from -0.1875 to 0.1875
- w_key: bfloat16 [1024, 128], replicated, may hold values from -0.1875 to 0.1875
- w_value: bfloat16 [1024, 128], replicated, may hold values from -0.1875 to 0.1875
- w_output: bfloat16 [512, 1024], P('tp'), may hold values from -0.25 to 0.25
- head_bias: float32 [8], replicated, may hold values from -9 to -2
- keys_cache: bfloat16 [2048, 1024, 128], P(('ep', 'tp')), may hold values from -6 to 6
- values_cache: bfloat16 [2048, 1024, 128], P(('ep', 'tp')), may hold values from -6 to 6
- lengths: int32 [2048], P(('ep', 'tp')), may hold values from 256 to 1024
- dense_gate_w: bfloat16 [4096, 1024], P('ep'), may hold values from -0.1875 to 0.1875
- dense_up_w: bfloat16 [4096, 1024], P('ep'), may hold values from -0.1875 to 0.1875
- dense_down_w: bfloat16 [4096, 1024], P('ep'), may hold values from -0.09375 to 0.09375
- mix_gate: bfloat16 [1024], replicated, may hold values from -0.1875 to 0.1875
- expert_gate: bfloat16 [128, 1024, 1024], P('ep', None, 'tp'), may hold values from -0.1875 to 0.1875
- expert_up: bfloat16 [128, 1024, 1024], P('ep', None, 'tp'), may hold values from -0.1875 to 0.1875
- expert_down: bfloat16 [128, 1024, 1024], P('ep', 'tp'), may hold values from -0.09375 to 0.09375
- routes: int32 [2048, 2], P(('ep', 'tp')), may hold values from 0 to 31, all different within a row; in each aligned block of 16 rows (0 to 15, 16 to 31, ...) at most 2 rows name the same one
- route_weights: float32 [2048, 2], P(('ep', 'tp')), may hold values from 0.1 to 0.9
Outputs:
- layer_out: bfloat16 [2048, 1024], P(('ep', 'tp'))
- new_keys: bfloat16 [2048, 128], P(('ep', 'tp'))
- new_values: bfloat16 [2048, 128], P(('ep', 'tp'))
Inputs may be any that keep to these rules, and one draw needn't show every extreme that they name: `routes`: each row names 2 different experts. In each aligned block of 16 rows (the tokens held by one index of ep) no expert is named by more than 2 rows, a bound that some block reaches.
All inputs are finite; a program needn't handle non-finite values.
Results may differ from a plain program's by a relative error of at most 0.01.
Values may be sent and summed in bfloat16 or wider, within the bound.
No kernel may reach another device: no remote copies, remote signals or barrier semaphores. Data moves between devices by JAX's collectives and lax.ppermute only.
A program may use at most 64 MiB of HBM per device.

v0:
```python
import math
import jax
import jax.numpy as jnp
from jax import lax
from jax.sharding import PartitionSpec as P

HEADS = 8
HEAD = 64
TOP = 2
SPLIT = 4
EPS = 1e-06


def laid_out(pieces, dim):
    pieces = jnp.moveaxis(pieces, 0, dim)
    lengths = pieces.shape
    return pieces.reshape(*lengths[:dim], lengths[dim] * lengths[dim + 1], *lengths[dim + 2 :])


def copy_for_each(array, axis):
    copies = jnp.broadcast_to(array, (lax.axis_size(axis), *array.shape))
    return lax.all_to_all(copies, axis, split_axis=0, concat_axis=0, tiled=True)


def collect(array, axis, dim):
    return laid_out(copy_for_each(array, axis), dim)


def split_up(array, dim, size):
    lengths = array.shape
    pieces = array.reshape(*lengths[:dim], size, lengths[dim] // size, *lengths[dim + 1 :])
    return jnp.moveaxis(pieces, dim, 0)


def sent_and_summed(array, axis, dim):
    size = lax.axis_size(axis)
    pieces = lax.all_to_all(split_up(array, dim, size), axis, 0, 0, tiled=True)
    return jnp.sum(pieces.astype(jnp.float32), axis=0)


def partner_2(block, axis, apart):
    count = lax.axis_size(axis)
    route = []
    for low in range(count):
        high = low | 1 << apart
        if high != low and high < count:
            route += [(low, high), (high, low)]
    return lax.ppermute(block, axis, route)


def rms_scale(values, gains):
    widened = values.astype(jnp.float32)
    scaled = widened * lax.rsqrt(jnp.mean(widened * widened, axis=-1, keepdims=True) + EPS)
    return (scaled * gains.astype(jnp.float32)).astype(jnp.bfloat16)


def slot_table(route_ids, experts_total, capacity):
    expert_ids = lax.broadcasted_iota(jnp.int32, route_ids.shape + (experts_total,), route_ids.ndim)
    picked = (route_ids[..., None] == expert_ids).astype(jnp.float32)
    chosen = jnp.sum(picked, axis=-2)
    earlier = jnp.cumsum(chosen, axis=-2) - chosen
    slot_ids = lax.broadcasted_iota(jnp.int32, chosen.shape + (capacity,), chosen.ndim).astype(
        jnp.float32
    )
    table = chosen[..., None] * (earlier[..., None] == slot_ids).astype(jnp.float32)
    return (picked, table)


def stick_read(queries, keys_cache, values_cache, lengths, head_bias):
    seq_count, positions, joined = keys_cache.shape
    kv_heads = joined // HEAD
    groups = HEADS // kv_heads
    query_heads = queries.reshape(seq_count, kv_heads, groups, HEAD)
    key_heads = keys_cache.reshape(seq_count, positions, kv_heads, HEAD)
    value_heads = values_cache.reshape(seq_count, positions, kv_heads, HEAD)
    scores = jnp.einsum(
        "bkgd,bpkd->bkgp", query_heads, key_heads, preferred_element_type=jnp.float32
    )
    scores = scores * (1.0 / math.sqrt(HEAD)) + head_bias.reshape(1, kv_heads, groups, 1)
    position = lax.broadcasted_iota(jnp.int32, scores.shape, 3)
    is_live = position < lengths.reshape(seq_count, 1, 1, 1)
    skipped = jnp.where(is_live, jax.nn.log_sigmoid(-scores), 0.0)
    later_sum = lax.cumsum(skipped, axis=3, reverse=True) - skipped
    weights = jnp.where(is_live, jnp.exp(jax.nn.log_sigmoid(scores) + later_sum), 0.0).astype(
        jnp.bfloat16
    )
    mixed_heads = jnp.einsum(
        "bkgp,bpkd->bkgd", weights, value_heads, preferred_element_type=jnp.float32
    )
    return mixed_heads.astype(jnp.bfloat16).reshape(seq_count, HEADS * HEAD)


def expert_rows(received, gate_local, up_local, down_local):
    dims_in = received.shape
    flat_rows = received.reshape(dims_in[0] * dims_in[1], dims_in[2])
    gate_val = jnp.dot(flat_rows, gate_local, preferred_element_type=jnp.float32)
    up_val = jnp.dot(flat_rows, up_local, preferred_element_type=jnp.float32)
    hidden = (jax.nn.silu(gate_val) * up_val).astype(jnp.bfloat16)
    result = jnp.dot(hidden, down_local, preferred_element_type=jnp.float32)
    return result.reshape(dims_in[0], dims_in[1], down_local.shape[1])


def body(
    tokens,
    gain_attn,
    gain_ffn,
    w_query,
    w_key,
    w_value,
    w_output,
    head_bias,
    keys_cache,
    values_cache,
    lengths,
    dense_gate_w,
    dense_up_w,
    dense_down_w,
    mix_gate,
    expert_gate,
    expert_up,
    expert_down,
    routes,
    route_weights,
):
    own_rows = tokens.shape[0]
    attn_in = rms_scale(tokens, gain_attn)
    query_group = jnp.dot(
        collect(attn_in, "tp", 0), w_query, preferred_element_type=jnp.float32
    ).astype(jnp.bfloat16)
    queries = lax.all_to_all(query_group, "tp", split_axis=0, concat_axis=1, tiled=True)
    new_keys = jnp.dot(attn_in, w_key, preferred_element_type=jnp.float32).astype(jnp.bfloat16)
    new_values = jnp.dot(attn_in, w_value, preferred_element_type=jnp.float32).astype(jnp.bfloat16)
    mixed_heads = stick_read(queries, keys_cache, values_cache, lengths, head_bias)
    heads_group = lax.all_to_all(mixed_heads, "tp", split_axis=1, concat_axis=0, tiled=True)
    attn_sum = sent_and_summed(
        jnp.dot(heads_group, w_output, preferred_element_type=jnp.float32).astype(jnp.bfloat16),
        "tp",
        0,
    )
    residual = (tokens.astype(jnp.float32) + attn_sum).astype(jnp.bfloat16)
    ffn_in = rms_scale(residual, gain_ffn)
    mix_scale = jax.nn.sigmoid(jnp.dot(ffn_in, mix_gate, preferred_element_type=jnp.float32))
    block_rows = lax.all_gather(ffn_in, "ep", axis=0, tiled=True)
    gate_val = jnp.dot(block_rows, dense_gate_w.T, preferred_element_type=jnp.float32)
    up_val = jnp.dot(block_rows, dense_up_w.T, preferred_element_type=jnp.float32)
    hidden_dense = (jax.nn.silu(gate_val) * up_val).astype(jnp.bfloat16)
    down_whole = lax.all_gather(dense_down_w, "ep", axis=0, tiled=True)
    hidden_own = lax.all_to_all(hidden_dense, "ep", split_axis=0, concat_axis=1, tiled=True)
    dense_out = jnp.dot(hidden_own, down_whole, preferred_element_type=jnp.float32)
    group_count = lax.axis_size("ep")
    group_rows = own_rows * lax.axis_size("tp")
    experts_total = group_count // SPLIT
    capacity = max(2, (group_rows * TOP + experts_total - 1) // experts_total)
    group_routes, group_weights = (
        lax.all_gather(routes, "tp", axis=0, tiled=True),
        lax.all_gather(route_weights, "tp", axis=0, tiled=True),
    )
    feature_part = lax.all_to_all(ffn_in, "tp", split_axis=1, concat_axis=0, tiled=True)
    picked, table = slot_table(group_routes, experts_total, capacity)
    weight_of = jnp.sum(group_weights[:, :, None] * picked, axis=1)
    quarter = jnp.einsum(
        "jxc,jd->xcd", table.astype(jnp.bfloat16), feature_part, preferred_element_type=jnp.float32
    ).astype(jnp.bfloat16)
    narrow = quarter.shape[2] // SPLIT
    pieces = (
        quarter.reshape(experts_total, capacity, SPLIT, narrow)
        .transpose(0, 2, 1, 3)
        .reshape(experts_total * SPLIT, capacity, narrow)
    )
    current = lax.all_to_all(pieces, "ep", split_axis=0, concat_axis=0, tiled=True)
    position = lax.axis_index("ep")
    for bit in range(SPLIT.bit_length() - 1):
        partner = partner_2(current, "ep", bit)
        upper = position // (1 << bit) % 2 == 1
        lower_half = jnp.where(upper, partner, current)
        upper_half = jnp.where(upper, current, partner)
        current = jnp.concatenate([lower_half, upper_half], axis=2)
    received = lax.all_gather(current, "tp", axis=2, tiled=True)
    partial_value = expert_rows(received, expert_gate[0], expert_up[0], expert_down[0])
    summed = sent_and_summed(partial_value.astype(jnp.bfloat16), "tp", 2)
    returned = lax.all_to_all(
        summed.astype(jnp.bfloat16), "ep", split_axis=0, concat_axis=0, tiled=True
    ).astype(summed.dtype)
    dims_back = returned.shape
    per_expert = jnp.sum(returned.reshape(experts_total, SPLIT, dims_back[1], dims_back[2]), axis=1)
    combine = table * weight_of[:, :, None]
    moe_group = jnp.einsum("jxc,xcd->jd", combine, per_expert, precision=lax.Precision.HIGHEST)
    moe_out = lax.all_to_all(moe_group, "tp", split_axis=0, concat_axis=1, tiled=True)
    layer_out = (residual.astype(jnp.float32) + moe_out + mix_scale[:, None] * dense_out).astype(
        jnp.bfloat16
    )
    return (layer_out, new_keys, new_values)


def solution(mesh):
    return jax.shard_map(
        body,
        mesh=mesh,
        in_specs=(
            P(("ep", "tp"), None),
            P(),
            P(),
            P(None, "tp"),
            P(),
            P(),
            P("tp", None),
            P(),
            P(("ep", "tp"), None, None),
            P(("ep", "tp"), None, None),
            P(("ep", "tp")),
            P("ep", None),
            P("ep", None),
            P("ep", None),
            P(),
            P("ep", None, "tp"),
            P("ep", None, "tp"),
            P("ep", "tp", None),
            P(("ep", "tp"), None),
            P(("ep", "tp"), None),
        ),
        out_specs=(P(("ep", "tp"), None), P(("ep", "tp"), None), P(("ep", "tp"), None)),
        check_vma=False,
    )
```

profile of v0, /device:TPU:1, one launch (start us, length us, event | category | flops | bytes accessed | tf_op | source)
XLA Modules:
  0.0 277.3 jit_solution(14062329265283297305)
XLA Ops:
  9.6 8.9 %all_to_all.114 = bf16[4,4,1024]{2,1,0:T(4,128)(2,1)S(1)} all-to-all(bf16[4,4,1024]{2,1,0:T(4,128)(2,1)S(1)} %broadcast_in_dim.5), channel_id=1, replica_groups=mesh['ep'=128,'tp'=4] {'tp'}, dimensions={0} | all-to-all | bytes 65536 | tf_op jit(solution)/shard_map/all_to_all | solution.py:22
  20.3 3.2 %all-to-all-start.1 = ((bf16[4,4,128]{2,1,0:T(4,128)(2,1)}), bf16[4,4,128]{2,1,0:T(4,128)(2,1)S(1)}, u32[]{:S(2)}, u32[]{:S(2)}) async-start(bf16[4,4,128]{2,1,0:T(4,128)(2,1)} %bitcast), calls=%async_computation.1 | async-start | bytes 8192 | tf_op jit(solution)/shard_map/all_to_all | solution.py:130
  30.2 39.6 %reduce-window.6 = f32[4,2,4,8,128]{4,3,2,1,0:T(8,128)S(1)} reduce-window(f32[4,2,4,8,128]{4,3,2,1,0:T(8,128)S(1)} %reshape.112, f32[]{:T(128)} %constant.60.clone.1), window={size=1x1x1x1x128 pad=0_0x0_0x0_0x0_0x0_127}, to_apply=%region_1.2 | reduce-window | flops 4161536 | bytes 262148 | tf_op jit(solution)/shard_map/reduce-window
  73.2 8.1 %all_to_all.115 = bf16[4,4,128]{2,0,1:T(4,128)(2,1)S(1)} all-to-all(bf16[4,4,128]{2,0,1:T(4,128)(2,1)S(1)} %copy.96), channel_id=1, replica_groups=mesh['ep'=128,'tp'=4] {'tp'}, dimensions={1} | all-to-all | bytes 8192 | tf_op jit(solution)/shard_map/all_to_all | solution.py:134
  82.1 3.3 %all-to-all-start.3 = ((bf16[4,4,1024]{2,1,0:T(4,128)(2,1)}), bf16[4,4,1024]{2,1,0:T(4,128)(2,1)S(1)}, u32[]{:S(2)}, u32[]{:S(2)}) async-start(bf16[4,4,1024]{2,1,0:T(4,128)(2,1)} %reshape.115), calls=%async_computation.3 | async-start | bytes 65536 | tf_op jit(solution)/shard_map/all_to_all | solution.py:37
  86.1 3.5 %all-to-all-done.3 = bf16[4,4,1024]{2,1,0:T(4,128)(2,1)S(1)} async-done(((bf16[4,4,1024]{2,1,0:T(4,128)(2,1)}), bf16[4,4,1024]{2,1,0:T(4,128)(2,1)S(1)}, u32[]{:S(2)}, u32[]{:S(2)}) %all-to-all-start.3) | async-done | bytes 32800 | tf_op jit(solution)/shard_map/all_to_all | solution.py:37
  91.3 6.5 %all-gather = s32[4,4,2]{1,2,0:T(2,128)S(1)} all-gather(s32[1,4,2]{1,2,0:T(2,128)} %bitcast.110), channel_id=1, replica_groups=mesh['ep'=128,'tp'=4] {'tp'}, dimensions={0}, use_global_device_ids=true | all-gather | bytes 160 | tf_op jit(solution)/shard_map/all_gather | solution.py:155
  97.8 6.4 %all-gather.1 = f32[4,4,2]{1,2,0:T(2,128)S(1)} all-gather(f32[1,4,2]{1,2,0:T(2,128)} %bitcast.111), channel_id=1, replica_groups=mesh['ep'=128,'tp'=4] {'tp'}, dimensions={0}, use_global_device_ids=true | all-gather | bytes 160 | tf_op jit(solution)/shard_map/all_gather | solution.py:156
  105.1 3.2 %all-to-all-start.4 = ((bf16[4,4,256]{2,0,1:T(4,128)(2,1)}), bf16[4,4,256]{2,0,1:T(4,128)(2,1)S(1)}, u32[]{:S(2)}, u32[]{:S(2)}) async-start(bf16[4,4,256]{2,0,1:T(4,128)(2,1)} %bitcast.11), calls=%async_computation.4 | async-start | bytes 16384 | tf_op jit(solution)/shard_map/all_to_all | solution.py:158
  108.4 4.1 %all-to-all-done.4 = bf16[4,4,256]{2,0,1:T(4,128)(2,1)S(1)} async-done(((bf16[4,4,256]{2,0,1:T(4,128)(2,1)}), bf16[4,4,256]{2,0,1:T(4,128)(2,1)S(1)}, u32[]{:S(2)}, u32[]{:S(2)}) %all-to-all-start.4) | async-done | bytes 8224 | tf_op jit(solution)/shard_map/all_to_all | solution.py:158
  112.9 37.9 %all_to_all.116 = bf16[128,2,64]{2,1,0:T(2,128)(2,1)S(1)} all-to-all(bf16[128,2,64]{2,1,0:T(2,128)(2,1)S(1)} %bitcast.101), channel_id=1, replica_groups=mesh['ep'=128,'tp'=4] {'ep'}, dimensions={0} | all-to-all | bytes 65536 | tf_op jit(solution)/shard_map/all_to_all | solution.py:170
  150.8 2.5 collective-permute-start
  154.4 2.4 collective-permute-start.1
  156.9 2.5 collective-permute-done.1
  159.8 9.9 %all_gather.17 = bf16[128,2,1024]{2,1,0:T(2,128)(2,1)S(1)} all-gather(bf16[128,2,256]{2,1,0:T(2,128)(2,1)S(1)} %pad_maximum_fusion), channel_id=1, replica_groups=mesh['ep'=128,'tp'=4] {'tp'}, dimensions={2}, use_global_device_ids=true | all-gather | bytes 655360 | tf_op jit(solution)/shard_map/all_gather | solution.py:178
  172.0 9.3 %all_to_all.117 = bf16[4,128,2,256]{3,1,2,0:T(8,128)(2,1)S(1)} all-to-all(bf16[4,128,2,256]{3,1,2,0:T(8,128)(2,1)S(1)} %bitcast.91), channel_id=1, replica_groups=mesh['ep'=128,'tp'=4] {'tp'}, dimensions={0} | all-to-all | bytes 1048576 | tf_op jit(solution)/shard_map/all_to_all | solution.py:37
  182.2 9.0 %all-to-all-start.7 = ((bf16[128,2,256]{2,1,0:T(2,128)(2,1)}), bf16[128,2,256]{2,1,0:T(2,128)(2,1)S(1)}, u32[]{:S(2)}, u32[]{:S(2)}) async-start(bf16[128,2,256]{2,1,0:T(2,128)(2,1)} %copy.104), calls=%async_computation.7 | async-start | bytes 262144 | tf_op jit(solution)/shard_map/all_to_all | solution.py:181
  192.8 11.7 %all-to-all-done.7 = bf16[128,2,256]{2,1,0:T(2,128)(2,1)S(1)} async-done(((bf16[128,2,256]{2,1,0:T(2,128)(2,1)}), bf16[128,2,256]{2,1,0:T(2,128)(2,1)S(1)}, u32[]{:S(2)}, u32[]{:S(2)}) %all-to-all-start.7) | async-done | bytes 131104 | tf_op jit(solution)/shard_map/all_to_all | solution.py:181
  207.6 5.7 %all-to-all-start.9 = ((bf16[128,4,32]{2,1,0:T(4,128)(2,1)}), bf16[128,4,32]{2,1,0:T(4,128)(2,1)S(1)}, u32[]{:S(2)}, u32[]{:S(2)}) async-start(bf16[128,4,32]{2,1,0:T(4,128)(2,1)} %bitcast.27), calls=%async_computation.9 | async-start | bytes 262144 | tf_op jit(solution)/shard_map/all_to_all | solution.py:148
  214.2 12.0 %all-to-all-done.9 = bf16[128,4,32]{2,1,0:T(4,128)(2,1)S(1)} async-done(((bf16[128,4,32]{2,1,0:T(4,128)(2,1)}), bf16[128,4,32]{2,1,0:T(4,128)(2,1)S(1)}, u32[]{:S(2)}, u32[]{:S(2)}) %all-to-all-start.9) | async-done | bytes 32800 | tf_op jit(solution)/shard_map/all_to_all | solution.py:148
  226.2 3.2 %all-to-all-start.8 = ((f32[4,4,256]{2,1,0:T(4,128)}), f32[4,4,256]{2,1,0:T(4,128)S(1)}, u32[]{:S(2)}, u32[]{:S(2)}) async-start(f32[4,4,256]{2,1,0:T(4,128)} %convolution_bitcast_fusion), calls=%async_computation.8 | async-start | bytes 32768 | tf_op jit(solution)/shard_map/all_to_all | solution.py:188
  230.5 3.1 %all-to-all-done.8 = f32[4,4,256]{2,1,0:T(4,128)S(1)} async-done(((f32[4,4,256]{2,1,0:T(4,128)}), f32[4,4,256]{2,1,0:T(4,128)S(1)}, u32[]{:S(2)}, u32[]{:S(2)}) %all-to-all-start.8) | async-done | bytes 16416 | tf_op jit(solution)/shard_map/all_to_all | solution.py:188
  233.7 31.7 %all-gather.6.cloned.1.call-done = bf16[4096,1024]{1,0:T(8,128)(2,1)} async-done(((bf16[32,1024]{1,0:T(8,128)(2,1)}), bf16[4096,1024]{1,0:T(8,128)(2,1)}) %all-gather.6.cloned.1.call-update) | async-done | bytes 8388624 | tf_op jit(solution)/shard_map/all_gather | solution.py:147
  265.3 5.2 %fusion.4 = bf16[4,1024]{1,0:T(4,128)(2,1)} fusion(bf16[4,4096]{1,0:T(4,128)(2,1)S(1)} %all_to_all.103, bf16[4096,1024]{1,0:T(8,128)(2,1)} %all-gather.6.cloned.1.call-done, f32[4,1024]{1,0:T(4,128)S(1)} %bitcast.105, bf16[4,1024]{1,0:T(4,128)(2,1)S(1)} %get-tuple-element.6, f32[4]{0:T(128)S(1)} %fusion.8), kind=kOutput, calls=%fused_computation.12 | convolution fusion | flops 33574912 | bytes 8454160 | tf_op jit(solution)/shard_map/dot_general | solution.py:149
  (93 shorter events, 29.7 us)
Async XLA Ops:
  7.2 164.5 %copy-start = (bf16[1,256,1024]{2,1,0:T(8,128)(2,1)S(1)}, bf16[1,256,1024]{2,1,0:T(8,128)(2,1)}, u32[]{:S(2)}) copy-start(bf16[1,256,1024]{2,1,0:T(8,128)(2,1)} %param.37) | copy-start | bytes 1572868
  7.2 82.5 %copy-start.5 = (bf16[4,1024]{1,0:T(4,128)(2,1)S(1)}, bf16[4,1024]{1,0:T(4,128)(2,1)}, u32[]{:S(2)}) copy-start(bf16[4,1024]{1,0:T(4,128)(2,1)} %param.20) | copy-start | bytes 24580
  7.2 74.2 %copy-start.2 = (bf16[128,1024]{1,0:T(8,128)(2,1)S(1)}, bf16[128,1024]{1,0:T(8,128)(2,1)}, u32[]{:S(2)}) copy-start(bf16[128,1024]{1,0:T(8,128)(2,1)} %param.26) | copy-start | bytes 786436
  7.2 162.7 %copy-start.1 = (bf16[1,1024,256]{2,1,0:T(8,128)(2,1)S(1)}, bf16[1,1024,256]{2,1,0:T(8,128)(2,1)}, u32[]{:S(2)}) copy-start(bf16[1,1024,256]{2,1,0:T(8,128)(2,1)} %param.35) | copy-start | bytes 1572868
  20.3 7.5 %all-to-all-start.1 = ((bf16[4,4,128]{2,1,0:T(4,128)(2,1)}), bf16[4,4,128]{2,1,0:T(4,128)(2,1)S(1)}, u32[]{:S(2)}, u32[]{:S(2)}) async-start(bf16[4,4,128]{2,1,0:T(4,128)(2,1)} %bitcast), calls=%async_computation.1 | async-start | bytes 8192 | tf_op jit(solution)/shard_map/all_to_all | solution.py:130
  30.1 161.1 %copy-start.3 = (bf16[1024,128]{1,0:T(8,128)(2,1)S(1)}, bf16[1024,128]{1,0:T(8,128)(2,1)}, u32[]{:S(2)}) copy-start(bf16[1024,128]{1,0:T(8,128)(2,1)} %param.25) | copy-start | bytes 786436
  30.1 161.9 %copy-start.8 = (bf16[1024]{0:T(1024)(128)(2,1)S(1)}, bf16[1024]{0:T(1024)(128)(2,1)}, u32[]{:S(2)}) copy-start(bf16[1024]{0:T(1024)(128)(2,1)} %param.34) | copy-start | bytes 6148
  30.2 161.9 %copy-start.4 = (bf16[1024,128]{1,0:T(8,128)(2,1)S(1)}, bf16[1024,128]{1,0:T(8,128)(2,1)}, u32[]{:S(2)}) copy-start(bf16[1024,128]{1,0:T(8,128)(2,1)} %param.24) | copy-start | bytes 786436
  71.6 134.4 %copy-start.6 = (bf16[32,1024]{1,0:T(8,128)(2,1)S(1)}, bf16[32,1024]{1,0:T(8,128)(2,1)}, u32[]{:S(2)}) copy-start(bf16[32,1024]{1,0:T(8,128)(2,1)} %param.31) | copy-start | bytes 196612
  73.1 133.3 %copy-start.7 = (bf16[32,1024]{1,0:T(8,128)(2,1)S(1)}, bf16[32,1024]{1,0:T(8,128)(2,1)}, u32[]{:S(2)}) copy-start(bf16[32,1024]{1,0:T(8,128)(2,1)} %param.32) | copy-start | bytes 196612
  82.1 7.5 %all-to-all-start.3 = ((bf16[4,4,1024]{2,1,0:T(4,128)(2,1)}), bf16[4,4,1024]{2,1,0:T(4,128)(2,1)S(1)}, u32[]{:S(2)}, u32[]{:S(2)}) async-start(bf16[4,4,1024]{2,1,0:T(4,128)(2,1)} %reshape.115), calls=%async_computation.3 | async-start | bytes 65536 | tf_op jit(solution)/shard_map/all_to_all | solution.py:37
  85.4 119.2 %all-gather.8.cloned.1.call-start = ((), (), s32[]{:S(2)}) async-start(), calls=%async_computation.11 | async-start | bytes 1056768 | tf_op jit(solution)/shard_map/all_gather | solution.py:143
  90.5 174.8 %all-gather.6.cloned.1.call-start = ((), (), s32[]{:S(2)}) async-start(), calls=%async_computation.10 | async-start | bytes 8454144 | tf_op jit(solution)/shard_map/all_gather | solution.py:147
  105.1 7.4 %all-to-all-start.4 = ((bf16[4,4,256]{2,0,1:T(4,128)(2,1)}), bf16[4,4,256]{2,0,1:T(4,128)(2,1)S(1)}, u32[]{:S(2)}, u32[]{:S(2)}) async-start(bf16[4,4,256]{2,0,1:T(4,128)(2,1)} %bitcast.11), calls=%async_computation.4 | async-start | bytes 16384 | tf_op jit(solution)/shard_map/all_to_all | solution.py:158
  150.8 3.3 %collective-permute-start = (bf16[128,2,64]{2,1,0:T(2,128)(2,1)S(1)}, bf16[128,2,64]{2,1,0:T(2,128)(2,1)S(1)}, u32[]{:S(2)}, u32[]{:S(2)}) collective-permute-start(bf16[128,2,64]{2,1,0:T(2,128)(2,1)S(1)} %all_to_all.116), channel_id=1, source_target_pairs={{0,4},{4,0},{8,12},{12,8},{16,20},{20,16},{24,28},{28,24},{32,36},... | collective-permute-start | bytes 98312 | tf_op jit(solution)/shard_map/ppermute | solution.py:48
  154.4 5.0 %collective-permute-start.1 = (bf16[128,2,128]{2,1,0:T(2,128)(2,1)S(1)}, bf16[128,2,128]{2,1,0:T(2,128)(2,1)S(1)}, u32[]{:S(2)}, u32[]{:S(2)}) collective-permute-start(bf16[128,2,128]{2,1,0:T(2,128)(2,1)S(1)} %pad_maximum_fusion.2), channel_id=1, source_target_pairs={{0,8},{8,0},{4,12},{12,4},{16,24},{24,16},{20,28},{28,20},{32,40},... | collective-permute-start | bytes 196616 | tf_op jit(solution)/shard_map/ppermute | solution.py:48
  182.2 22.2 %all-to-all-start.7 = ((bf16[128,2,256]{2,1,0:T(2,128)(2,1)}), bf16[128,2,256]{2,1,0:T(2,128)(2,1)S(1)}, u32[]{:S(2)}, u32[]{:S(2)}) async-start(bf16[128,2,256]{2,1,0:T(2,128)(2,1)} %copy.104), calls=%async_computation.7 | async-start | bytes 262144 | tf_op jit(solution)/shard_map/all_to_all | solution.py:181
  207.6 18.6 %all-to-all-start.9 = ((bf16[128,4,32]{2,1,0:T(4,128)(2,1)}), bf16[128,4,32]{2,1,0:T(4,128)(2,1)S(1)}, u32[]{:S(2)}, u32[]{:S(2)}) async-start(bf16[128,4,32]{2,1,0:T(4,128)(2,1)} %bitcast.27), calls=%async_computation.9 | async-start | bytes 262144 | tf_op jit(solution)/shard_map/all_to_all | solution.py:148
  226.2 7.4 %all-to-all-start.8 = ((f32[4,4,256]{2,1,0:T(4,128)}), f32[4,4,256]{2,1,0:T(4,128)S(1)}, u32[]{:S(2)}, u32[]{:S(2)}) async-start(f32[4,4,256]{2,1,0:T(4,128)} %convolution_bitcast_fusion), calls=%async_computation.8 | async-start | bytes 32768 | tf_op jit(solution)/shard_map/all_to_all | solution.py:188
Sparse Core Ops, SparseCore 0:
  90.7 86.9 all-gather.7
  180.8 84.4 all-gather.5
where the time goes:
time: 278 us; the launch traced here: 277 us
  blocking collectives  87.1 us (31%)
  waiting for transfers between devices  70.3 us (25%)
  other arithmetic  46.7 us (17%)
  starting transfers between devices  32.7 us (12%)
  matrix products  16.3 us (6%)
  between operations  14.4 us (5%)
  local copies, waits for them, and re-layouts  9.8 us (4%)
    another operation x2, other arithmetic  41.1 us
    all_to_all x1, blocking collectives, body(): lax.all_to_all(pieces, 'ep', split_axis=0, concat_axis=0, tiled=True)  37.9 us
    all_gather x1, waiting for transfers between devices, body(): down_whole = lax.all_gather(dense_down_w, 'ep', axis=0, tiled=True)  31.7 us
    all_to_all x1, waiting for transfers between devices, body(): lax.all_to_all(hidden_dense, 'ep', split_axis=0, concat_axis=1, tiled=True)  12 us
    all_to_all x1, waiting for transfers between devices, body(): lax.all_to_all(summed.astype(jnp.bfloat16), 'ep', split_axis=0, concat_ax...  11.7 us
    all_gather x1, blocking collectives, body(): received = lax.all_gather(current, 'tp', axis=2, tiled=True)  9.95 us
    all_to_all x1, blocking collectives, sent_and_summed(): pieces = lax.all_to_all(split_up(array, dim, size), axis, 0, 0, tiled=True)  9.33 us
    all_to_all x1, starting transfers between devices, body(): lax.all_to_all(summed.astype(jnp.bfloat16), 'ep', split_axis=0, concat_ax...  9.04 us
  transfers between devices with their start and end apart: 10, of which 8 were waited for; matrix products, arithmetic and copies ran while one was open for 6% of the time, Pallas kernels for 0%

commit v1 on v0

--- a/solution.py
+++ b/solution.py
@@ -9,6 +9,13 @@
 TOP = 2
 SPLIT = 4
 EPS = 1e-06
+
+
+def swapped_in(shard, axis, along):
+    size = lax.axis_size(axis)
+    blocks = jnp.stack([shard for _ in range(size)])
+    blocks = lax.all_to_all(blocks, axis, split_axis=0, concat_axis=0)
+    return jnp.concatenate(blocks, axis=along)
 
 
 def laid_out(pieces, dim):
@@ -144,7 +151,7 @@
     gate_val = jnp.dot(block_rows, dense_gate_w.T, preferred_element_type=jnp.float32)
     up_val = jnp.dot(block_rows, dense_up_w.T, preferred_element_type=jnp.float32)
     hidden_dense = (jax.nn.silu(gate_val) * up_val).astype(jnp.bfloat16)
-    down_whole = lax.all_gather(dense_down_w, "ep", axis=0, tiled=True)
+    down_whole = swapped_in(dense_down_w, "ep", 0)
     hidden_own = lax.all_to_all(hidden_dense, "ep", split_axis=0, concat_axis=1, tiled=True)
     dense_out = jnp.dot(hidden_own, down_whole, preferred_element_type=jnp.float32)
     group_count = lax.axis_size("ep")

time: 278 us -> 526 us (1.89)
  the two profiles are of different devices: /device:TPU:1 before, /device:TPU:17 now
where the time goes in v1:
time: 526 us; the launch traced here: 525 us
  waiting for transfers between devices  296 us (56%)
  blocking collectives  96.1 us (18%)
  other arithmetic  46.7 us (9%)
  starting transfers between devices  41.9 us (8%)
  matrix products  15.4 us (3%)
  between operations  14.5 us (3%)
  local copies, waits for them, and re-layouts  13.8 us (3%)
    all_to_all x1, waiting for transfers between devices, swapped_in(): blocks = lax.all_to_all(blocks, axis, split_axis=0, concat_axis=0)  253 us
    another operation x2, other arithmetic  41.1 us
    all_to_all x1, blocking collectives, body(): lax.all_to_all(pieces, 'ep', split_axis=0, concat_axis=0, tiled=True)  35.5 us
    all_gather x1, waiting for transfers between devices, body(): block_rows = lax.all_gather(ffn_in, 'ep', axis=0, tiled=True)  21.8 us
    all_to_all x1, blocking collectives, body(): lax.all_to_all(hidden_dense, 'ep', split_axis=0, concat_axis=1, tiled=True)  20.4 us
    all_to_all x1, starting transfers between devices, body(): lax.all_to_all(summed.astype(jnp.bfloat16), 'ep', split_axis=0, concat_ax...  11.3 us
    all_to_all x1, waiting for transfers between devices, body(): lax.all_to_all(summed.astype(jnp.bfloat16), 'ep', split_axis=0, concat_ax...  10.9 us
  transfers between devices with their start and end apart: 10, of which 7 were waited for; matrix products, arithmetic and copies ran while one was open for 3% of the time, Pallas kernels for 0%

profile of v1, /device:TPU:17, one launch (start us, length us, event | category | flops | bytes accessed | tf_op | source)
XLA Modules:
  0.0 524.5 jit_solution(2146650487934912620)
XLA Ops:
  9.6 8.1 %all_to_all.116 = bf16[4,4,1024]{2,1,0:T(4,128)(2,1)S(1)} all-to-all(bf16[4,4,1024]{2,1,0:T(4,128)(2,1)S(1)} %broadcast_in_dim.5), channel_id=1, replica_groups=mesh['ep'=128,'tp'=4] {'tp'}, dimensions={0} | all-to-all | bytes 65536 | tf_op jit(solution)/shard_map/all_to_all | solution.py:29
  19.4 3.2 all-to-all-start.1
  29.4 39.6 %reduce-window.6 = f32[4,2,4,8,128]{4,3,2,1,0:T(8,128)S(1)} reduce-window(f32[4,2,4,8,128]{4,3,2,1,0:T(8,128)S(1)} %reshape.115, f32[]{:T(128)} %constant.60.clone.1), window={size=1x1x1x1x128 pad=0_0x0_0x0_0x0_0x0_127}, to_apply=%region_1.2 | reduce-window | flops 4161536 | bytes 262148 | tf_op jit(solution)/shard_map/reduce-window
  73.0 4.2 all-to-all-start.2
  77.2 8.1 %all-gather.1 = f32[4,4,2]{1,2,0:T(2,128)S(1)} all-gather(f32[1,4,2]{1,2,0:T(2,128)} %bitcast.119), channel_id=1, replica_groups=mesh['ep'=128,'tp'=4] {'tp'}, dimensions={0}, use_global_device_ids=true | all-gather | bytes 160 | tf_op jit(solution)/shard_map/all_gather | solution.py:163
  85.3 5.6 %all-gather = s32[4,4,2]{1,2,0:T(2,128)S(1)} all-gather(s32[1,4,2]{1,2,0:T(2,128)} %bitcast.120), channel_id=1, replica_groups=mesh['ep'=128,'tp'=4] {'tp'}, dimensions={0}, use_global_device_ids=true | all-gather | bytes 160 | tf_op jit(solution)/shard_map/all_gather | solution.py:162
  91.8 3.3 all-to-all-start.3
  95.9 3.5 all-to-all-done.3
  100.2 3.2 all-to-all-start.4
  103.6 4.0 all-to-all-done.4
  108.0 35.5 %all_to_all.117 = bf16[128,2,64]{2,1,0:T(2,128)(2,1)S(1)} all-to-all(bf16[128,2,64]{2,1,0:T(2,128)(2,1)S(1)} %bitcast.110), channel_id=1, replica_groups=mesh['ep'=128,'tp'=4] {'ep'}, dimensions={0} | all-to-all | bytes 65536 | tf_op jit(solution)/shard_map/all_to_all | solution.py:177
  143.5 2.5 collective-permute-start
  147.1 2.3 collective-permute-start.1
  152.5 9.0 %all_gather.14 = bf16[128,2,1024]{2,1,0:T(2,128)(2,1)S(1)} all-gather(bf16[128,2,256]{2,1,0:T(2,128)(2,1)S(1)} %pad_maximum_fusion), channel_id=1, replica_groups=mesh['ep'=128,'tp'=4] {'tp'}, dimensions={2}, use_global_device_ids=true | all-gather | bytes 655360 | tf_op jit(solution)/shard_map/all_gather | solution.py:185
  162.9 9.3 %all_to_all.118 = bf16[4,128,2,256]{3,1,2,0:T(8,128)(2,1)S(1)} all-to-all(bf16[4,128,2,256]{3,1,2,0:T(8,128)(2,1)S(1)} %bitcast.100), channel_id=1, replica_groups=mesh['ep'=128,'tp'=4] {'tp'}, dimensions={0} | all-to-all | bytes 1048576 | tf_op jit(solution)/shard_map/all_to_all | solution.py:44
  173.1 11.3 %all-to-all-start.7 = ((bf16[128,2,256]{2,1,0:T(2,128)(2,1)}), bf16[128,2,256]{2,1,0:T(2,128)(2,1)S(1)}, u32[]{:S(2)}, u32[]{:S(2)}) async-start(bf16[128,2,256]{2,1,0:T(2,128)(2,1)} %copy.105), calls=%async_computation.7 | async-start | bytes 262144 | tf_op jit(solution)/shard_map/all_to_all | solution.py:188
  184.4 10.9 %all-to-all-done.7 = bf16[128,2,256]{2,1,0:T(2,128)(2,1)S(1)} async-done(((bf16[128,2,256]{2,1,0:T(2,128)(2,1)}), bf16[128,2,256]{2,1,0:T(2,128)(2,1)S(1)}, u32[]{:S(2)}, u32[]{:S(2)}) %all-to-all-start.7) | async-done | bytes 131104 | tf_op jit(solution)/shard_map/all_to_all | solution.py:188
  196.3 3.2 all-to-all-start.8
  199.6 21.8 %all-gather.5.cloned.1.call-done = bf16[128,4,1024]{2,1,0:T(4,128)(2,1)} async-done(((bf16[1,4,1024]{2,1,0:T(4,128)(2,1)}), bf16[128,4,1024]{2,1,0:T(4,128)(2,1)}) %all-gather.5.cloned.1.call-update) | async-done | bytes 1048592 | tf_op jit(solution)/shard_map/all_gather | solution.py:150
  223.7 20.4 %all_to_all.119 = bf16[128,4,32]{2,1,0:T(4,128)(2,1)S(1)} all-to-all(bf16[128,4,32]{2,1,0:T(4,128)(2,1)S(1)} %bitcast.107), channel_id=1, replica_groups=mesh['ep'=128,'tp'=4] {'ep'}, dimensions={0} | all-to-all | bytes 65536 | tf_op jit(solution)/shard_map/all_to_all | solution.py:155
  244.1 4.3 stack.2
  248.4 8.6 %all-to-all-start.10 = ((bf16[128,32,1024]{2,1,0:T(8,128)(2,1)}), bf16[128,32,1024]{2,1,0:T(8,128)(2,1)}, u32[]{:S(2)}, u32[]{:S(2)}) async-start(bf16[128,32,1024]{2,1,0:T(8,128)(2,1)} %stack.2), calls=%async_computation.10 | async-start | bytes 16777216 | tf_op jit(solution)/shard_map/all_to_all | solution.py:17
  259.3 253.2 %all-to-all-done.10 = bf16[128,32,1024]{2,1,0:T(8,128)(2,1)} async-done(((bf16[128,32,1024]{2,1,0:T(8,128)(2,1)}), bf16[128,32,1024]{2,1,0:T(8,128)(2,1)}, u32[]{:S(2)}, u32[]{:S(2)}) %all-to-all-start.10) | async-done | bytes 8388640 | tf_op jit(solution)/shard_map/all_to_all | solution.py:17
  512.4 5.3 %fusion.5 = bf16[4,1024]{1,0:T(4,128)(2,1)} fusion(bf16[128,32,1024]{2,1,0:T(8,128)(2,1)} %all-to-all-done.10, bf16[128,4,32]{2,1,0:T(4,128)(2,1)S(1)} %all_to_all.119, f32[4,1024]{1,0:T(4,128)S(1)} %bitcast.113, bf16[4,1024]{1,0:T(4,128)(2,1)S(1)} %get-tuple-element.6, f32[4]{0:T(128)S(1)} %fusion.9), kind=kOutput, calls=%fused_computation.13 | convolution fusion | flops 33574912 | bytes 8454160 | tf_op jit(solution)/shard_map/dot_general | solution.py:156
  (95 shorter events, 29.6 us)
Async XLA Ops:
  7.2 155.3 %copy-start = (bf16[1,256,1024]{2,1,0:T(8,128)(2,1)S(1)}, bf16[1,256,1024]{2,1,0:T(8,128)(2,1)}, u32[]{:S(2)}) copy-start(bf16[1,256,1024]{2,1,0:T(8,128)(2,1)} %param.37) | copy-start | bytes 1572868
  7.2 92.2 %copy-start.5 = (bf16[4,1024]{1,0:T(4,128)(2,1)S(1)}, bf16[4,1024]{1,0:T(4,128)(2,1)}, u32[]{:S(2)}) copy-start(bf16[4,1024]{1,0:T(4,128)(2,1)} %param.20) | copy-start | bytes 24580
  7.2 83.9 %copy-start.2 = (bf16[128,1024]{1,0:T(8,128)(2,1)S(1)}, bf16[128,1024]{1,0:T(8,128)(2,1)}, u32[]{:S(2)}) copy-start(bf16[128,1024]{1,0:T(8,128)(2,1)} %param.26) | copy-start | bytes 786436
  7.2 154.6 %copy-start.1 = (bf16[1,1024,256]{2,1,0:T(8,128)(2,1)S(1)}, bf16[1,1024,256]{2,1,0:T(8,128)(2,1)}, u32[]{:S(2)}) copy-start(bf16[1,1024,256]{2,1,0:T(8,128)(2,1)} %param.35) | copy-start | bytes 1572868
  19.4 7.5 %all-to-all-start.1 = ((bf16[4,4,128]{2,1,0:T(4,128)(2,1)}), bf16[4,4,128]{2,1,0:T(4,128)(2,1)S(1)}, u32[]{:S(2)}, u32[]{:S(2)}) async-start(bf16[4,4,128]{2,1,0:T(4,128)(2,1)} %bitcast), calls=%async_computation.1 | async-start | bytes 8192 | tf_op jit(solution)/shard_map/all_to_all | solution.py:137
  29.3 132.8 %copy-start.10 = (bf16[1,1024,256]{2,1,0:T(8,128)(2,1)S(1)}, bf16[1,1024,256]{2,1,0:T(8,128)(2,1)}, u32[]{:S(2)}) copy-start(bf16[1,1024,256]{2,1,0:T(8,128)(2,1)} %param.36) | copy-start | bytes 1572868
  70.8 151.8 %copy-start.7 = (bf16[32,1024]{1,0:T(8,128)(2,1)S(1)}, bf16[32,1024]{1,0:T(8,128)(2,1)}, u32[]{:S(2)}) copy-start(bf16[32,1024]{1,0:T(8,128)(2,1)} %param.31) | copy-start | bytes 196612
  72.3 150.8 %copy-start.8 = (bf16[32,1024]{1,0:T(8,128)(2,1)S(1)}, bf16[32,1024]{1,0:T(8,128)(2,1)}, u32[]{:S(2)}) copy-start(bf16[32,1024]{1,0:T(8,128)(2,1)} %param.32) | copy-start | bytes 196612
  73.0 18.1 %all-to-all-start.2 = ((bf16[4,4,128]{2,0,1:T(4,128)(2,1)}), bf16[4,4,128]{2,0,1:T(4,128)(2,1)S(1)}, u32[]{:S(2)}, u32[]{:S(2)}) async-start(bf16[4,4,128]{2,0,1:T(4,128)(2,1)} %copy.97), calls=%async_computation.2 | async-start | bytes 8192 | tf_op jit(solution)/shard_map/all_to_all | solution.py:141
  91.8 7.5 %all-to-all-start.3 = ((bf16[4,4,1024]{2,1,0:T(4,128)(2,1)}), bf16[4,4,1024]{2,1,0:T(4,128)(2,1)S(1)}, u32[]{:S(2)}, u32[]{:S(2)}) async-start(bf16[4,4,1024]{2,1,0:T(4,128)(2,1)} %reshape.118), calls=%async_computation.3 | async-start | bytes 65536 | tf_op jit(solution)/shard_map/all_to_all | solution.py:44
  100.2 7.4 %all-to-all-start.4 = ((bf16[4,4,256]{2,0,1:T(4,128)(2,1)}), bf16[4,4,256]{2,0,1:T(4,128)(2,1)S(1)}, u32[]{:S(2)}, u32[]{:S(2)}) async-start(bf16[4,4,256]{2,0,1:T(4,128)(2,1)} %bitcast.11), calls=%async_computation.4 | async-start | bytes 16384 | tf_op jit(solution)/shard_map/all_to_all | solution.py:165
  103.5 117.8 %all-gather.5.cloned.1.call-start = ((), (), s32[]{:S(2)}) async-start(), calls=%async_computation.11 | async-start | bytes 1056768 | tf_op jit(solution)/shard_map/all_gather | solution.py:150
  108.0 136.1 %copy-start.6 = (bf16[32,1024]{1,0:T(8,128)(2,1)S(1)}, bf16[32,1024]{1,0:T(8,128)(2,1)}, u32[]{:S(2)}) copy-start(bf16[32,1024]{1,0:T(8,128)(2,1)} %param.33) | copy-start | bytes 196612
  143.5 3.4 collective-permute-start
  147.1 5.0 collective-permute-start.1
  173.1 22.2 %all-to-all-start.7 = ((bf16[128,2,256]{2,1,0:T(2,128)(2,1)}), bf16[128,2,256]{2,1,0:T(2,128)(2,1)S(1)}, u32[]{:S(2)}, u32[]{:S(2)}) async-start(bf16[128,2,256]{2,1,0:T(2,128)(2,1)} %copy.105), calls=%async_computation.7 | async-start | bytes 262144 | tf_op jit(solution)/shard_map/all_to_all | solution.py:188
  196.3 27.3 %all-to-all-start.8 = ((f32[4,4,256]{2,1,0:T(4,128)}), f32[4,4,256]{2,1,0:T(4,128)S(1)}, u32[]{:S(2)}, u32[]{:S(2)}) async-start(f32[4,4,256]{2,1,0:T(4,128)} %convolution_bitcast_fusion.1), calls=%async_computation.8 | async-start | bytes 32768 | tf_op jit(solution)/shard_map/all_to_all | solution.py:195
  248.4 8.6 %copy-start.9 = (bf16[1024]{0:T(1024)(128)(2,1)S(1)}, bf16[1024]{0:T(1024)(128)(2,1)}, u32[]{:S(2)}) copy-start(bf16[1024]{0:T(1024)(128)(2,1)} %param.34) | copy-start | bytes 6148
  248.4 8.6 %copy-start.3 = (bf16[1024,128]{1,0:T(8,128)(2,1)S(1)}, bf16[1024,128]{1,0:T(8,128)(2,1)}, u32[]{:S(2)}) copy-start(bf16[1024,128]{1,0:T(8,128)(2,1)} %param.24) | copy-start | bytes 786436
  248.4 9.3 %copy-start.4 = (bf16[1024,128]{1,0:T(8,128)(2,1)S(1)}, bf16[1024,128]{1,0:T(8,128)(2,1)}, u32[]{:S(2)}) copy-start(bf16[1024,128]{1,0:T(8,128)(2,1)} %param.25) | copy-start | bytes 786436
  248.4 264.0 %all-to-all-start.10 = ((bf16[128,32,1024]{2,1,0:T(8,128)(2,1)}), bf16[128,32,1024]{2,1,0:T(8,128)(2,1)}, u32[]{:S(2)}, u32[]{:S(2)}) async-start(bf16[128,32,1024]{2,1,0:T(8,128)(2,1)} %stack.2), calls=%async_computation.10 | async-start | bytes 16777216 | tf_op jit(solution)/shard_map/all_to_all | solution.py:17
Sparse Core Ops, SparseCore 0:
  150.3 70.9 all-gather.4
